TPU v7x, 32 devices: a whole 2x2x4 slice. The times are simulated.
32 devices in a mesh: gr: 2 (over core), sp: 8 (over z, y), tp: 2 (over x).
Axes of the slice: x: 2, y: 2, z: 4, core: 2. Of those that a mesh axis runs over, the one named last changes fastest.
Arguments:
- mixer_input: bfloat16 [16, 1536, 2048], P(('gr', 'tp'), 'sp'), may hold values from -16.8 to 16.8
- key_weight: bfloat16 [2048, 256], P('tp'), may hold values from -0.125 to 0.125
- content_projection_matrix: bfloat16 [2048, 256], P('tp'), may hold values from -0.125 to 0.125
- new_queries: bfloat16 [16, 32, 64], P(('gr', 'sp'), 'tp'), may hold values from -6 to 6
- head_stick_offset: float32 [32], replicated, may hold values from -11 to -4
Outputs:
- kv_cache: bfloat16 [16, 4, 1536, 128], P(('gr', 'sp'), 'tp')
- initial_attended_output: bfloat16 [16, 32, 64], P(('gr', 'sp'), 'tp')
All inputs are finite; a program needn't handle non-finite values.
Results may differ from a plain program's by a relative error of at most 0.0081.
Values may be sent and summed in bfloat16 or wider, within the bound.
A program may use at most 64 MiB of HBM per device.

v0:
```python
import jax
import jax.numpy as jnp
from jax import lax
from jax.sharding import PartitionSpec as P

HEAD_DIM = 64


def local(mixer_input, key_weight, content_projection_matrix, new_queries, head_stick_offset):
    group_seqs, block_rows, model_width = mixer_input.shape
    key_heads = key_weight.shape[1] // HEAD_DIM
    head_devices = lax.axis_size("tp")
    copies = max(1, head_devices // key_heads)
    input_rows = mixer_input.reshape(group_seqs * block_rows, model_width)
    key_sum = jnp.dot(
        input_rows,
        lax.all_gather(key_weight, "tp", axis=0, tiled=True),
        preferred_element_type=jnp.float32,
    )
    value_sum = jnp.dot(
        input_rows,
        lax.all_gather(content_projection_matrix, "tp", axis=0, tiled=True),
        preferred_element_type=jnp.float32,
    )
    key_rows = key_sum.astype(jnp.bfloat16).reshape(group_seqs, block_rows, key_heads, HEAD_DIM)
    value_rows = value_sum.astype(jnp.bfloat16).reshape(group_seqs, block_rows, key_heads, HEAD_DIM)
    stacked = jnp.concatenate([key_rows, value_rows], axis=3).transpose(0, 2, 1, 3)
    spread = jnp.repeat(stacked, copies, axis=1)
    spread = lax.all_to_all(spread, "tp", split_axis=1, concat_axis=0, tiled=True)
    kv_cache = lax.all_to_all(spread, "sp", split_axis=0, concat_axis=2, tiled=True)
    seq_local = kv_cache.shape[0]
    slot_local = kv_cache.shape[1]
    head_local = new_queries.shape[1]
    inverse_root = HEAD_DIM ** (-0.5)
    offset_values = lax.dynamic_slice_in_dim(
        head_stick_offset, lax.axis_index("tp") * head_local, head_local
    )
    grouped = new_queries.reshape(seq_local, slot_local, head_local // slot_local, HEAD_DIM)
    cache_keys = kv_cache[:, :, :, :HEAD_DIM]
    cache_values = kv_cache[:, :, :, HEAD_DIM:]
    logit_scores = (
        jnp.einsum("bhgd,bhsd->bhgs", grouped, cache_keys, preferred_element_type=jnp.float32)
        * inverse_root
    )
    logit_scores = logit_scores + offset_values.reshape(1, slot_local, -1, 1)
    stay_terms = jax.nn.log_sigmoid(-logit_scores)
    later_terms = lax.cumsum(stay_terms, axis=3, reverse=True) - stay_terms
    weights = jnp.exp(jax.nn.log_sigmoid(logit_scores) + later_terms).astype(jnp.bfloat16)
    result = jnp.einsum(
        "bhgs,bhsd->bhgd", weights, cache_values, preferred_element_type=jnp.float32
    )
    initial_attended_output = result.reshape(seq_local, head_local, HEAD_DIM).astype(jnp.bfloat16)
    return (kv_cache, initial_attended_output)


def solution(mesh):
    return jax.shard_map(
        local,
        mesh=mesh,
        in_specs=(
            P(("gr", "tp"), "sp", None),
            P("tp", None),
            P("tp", None),
            P(("gr", "sp"), "tp", None),
            P(),
        ),
        out_specs=(P(("gr", "sp"), "tp", None, None), P(("gr", "sp"), "tp", None)),
        check_vma=False,
    )
```

profile of v0, /device:TPU:0, one launch (start us, length us, event | category | flops | bytes accessed | tf_op | source)
XLA Modules:
  0.0 139.1 jit_solution(8693301563375391553)
XLA Ops:
  7.2 0.0 copy-start
  7.2 0.0 all-gather.5.cloned.1.call-start
  7.2 0.7 all-gather.5.cloned.1.call-update
  7.9 0.0 all-gather.3.cloned.1.call-start
  8.0 0.7 all-gather.3.cloned.1.call-update
  8.7 24.9 %all-gather.5.cloned.1.call-done = bf16[2048,256]{1,0:T(8,128)(2,1)} async-done(((bf16[1024,256]{1,0:T(8,128)(2,1)}), bf16[2048,256]{1,0:T(8,128)(2,1)}) %all-gather.5.cloned.1.call-update) | async-done | bytes 1048592 | tf_op jit(solution)/shard_map/all_gather | solution.py:22
  33.6 0.0 copy-done
  33.6 3.0 %convolution_convert_fusion = bf16[768,256]{1,0:T(8,128)(2,1)} fusion(bf16[768,2048]{1,0:T(8,128)(2,1)S(1)} %bitcast.47, bf16[2048,256]{1,0:T(8,128)(2,1)} %all-gather.5.cloned.1.call-done), kind=kOutput, calls=%fused_computation.3 | convolution fusion | flops 805502976 | bytes 4587520 | tf_op jit(solution)/shard_map/dot_general | solution.py:20
  36.5 1.2 copy.28
  37.7 1.3 reshape.94
  39.0 17.5 %all-gather.3.cloned.1.call-done = bf16[2048,256]{1,0:T(8,128)(2,1)} async-done(((bf16[1024,256]{1,0:T(8,128)(2,1)}), bf16[2048,256]{1,0:T(8,128)(2,1)}) %all-gather.3.cloned.1.call-update) | async-done | bytes 1048592 | tf_op jit(solution)/shard_map/all_gather | solution.py:17
  56.4 3.0 %convolution_convert_fusion.1 = bf16[768,256]{1,0:T(8,128)(2,1)} fusion(bf16[768,2048]{1,0:T(8,128)(2,1)S(1)} %bitcast.46, bf16[2048,256]{1,0:T(8,128)(2,1)} %all-gather.3.cloned.1.call-done), kind=kOutput, calls=%fused_computation.4 | convolution fusion | flops 805502976 | bytes 4587520 | tf_op jit(solution)/shard_map/dot_general | solution.py:15
  59.4 1.2 copy.27
  60.6 1.3 reshape.93
  61.8 2.9 %maximum_bitcast_fusion = bf16[4,4,192,128]{2,0,3,1:T(4,128)(2,1)} fusion(bf16[4,192,4,64]{1,0,3,2:T(4,128)(2,1)} %reshape.94, bf16[4,192,4,64]{1,0,3,2:T(4,128)(2,1)} %reshape.93), kind=kLoop, calls=%fused_computation.7 | loop fusion | flops 393216 | bytes 1572864 | tf_op jit(solution)/shard_map/transpose | solution.py:27
  64.8 0.0 copy-start.3
  64.8 2.3 %copy.29 = bf16[4,4,192,128]{3,2,0,1:T(8,128)(2,1)} copy(bf16[4,4,192,128]{2,0,3,1:T(4,128)(2,1)} %maximum_bitcast_fusion) | data formatting | bytes 1572864 | tf_op jit(solution)/shard_map/transpose | solution.py:27
  67.1 0.0 copy-start.2
  67.1 14.5 %all_to_all.36 = bf16[4,4,192,128]{3,2,0,1:T(8,128)(2,1)S(1)} all-to-all(bf16[4,4,192,128]{3,2,0,1:T(8,128)(2,1)} %copy.29), channel_id=1, replica_groups=mesh['gr'=2,'sp'=8,'tp'=2] {'tp'}, dimensions={1} | all-to-all | bytes 1572864 | tf_op jit(solution)/shard_map/all_to_all | solution.py:29
  81.6 0.9 copy.31
  82.6 5.5 %all-to-all-start.1 = ((bf16[8,2,192,128]{3,2,1,0:T(8,128)(2,1)}), bf16[8,2,192,128]{3,2,1,0:T(8,128)(2,1)}, u32[]{:S(2)}, u32[]{:S(2)}) async-start(bf16[8,2,192,128]{3,2,1,0:T(8,128)(2,1)} %bitcast.48), calls=%async_computation.1 | async-start | bytes 1572864 | tf_op jit(solution)/shard_map/all_to_all | solution.py:30
  88.1 0.0 copy-done.3
  88.1 0.1 dynamic_slice.3
  88.2 0.1 add.32
  88.3 19.2 %all-to-all-done.1 = bf16[8,2,192,128]{3,2,1,0:T(8,128)(2,1)} async-done(((bf16[8,2,192,128]{3,2,1,0:T(8,128)(2,1)}), bf16[8,2,192,128]{3,2,1,0:T(8,128)(2,1)}, u32[]{:S(2)}, u32[]{:S(2)}) %all-to-all-start.1) | async-done | bytes 786464 | tf_op jit(solution)/shard_map/all_to_all | solution.py:30
  107.4 1.2 copy.32
  108.6 0.0 copy-start.1
  108.6 0.0 copy-done.2
  108.6 0.3 fusion.1
  108.9 0.1 fusion.13
  109.0 0.5 copy-done.1
  109.5 19.9 %reduce-window.6 = f32[1,2,8,12,128]{4,3,2,1,0:T(8,128)S(1)} reduce-window(f32[1,2,8,12,128]{4,3,2,1,0:T(8,128)S(1)} %copy.34, f32[]{:T(128)} %constant.18.clone.1), window={size=1x1x1x1x128 pad=0_0x0_0x0_0x0_0x0_127}, to_apply=%region_0.1 | reduce-window | flops 3121152 | bytes 196612 | tf_op jit(solution)/shard_map/reduce-window
  129.4 0.1 slice_reduce_fusion
  129.5 0.3 reduce-window.9
  129.9 0.1 slice_bitcast_fusion.4
  129.9 0.1 copy.35
  130.0 2.2 %fusion.2 = bf16[1,16,64]{2,1,0:T(8,128)(2,1)} fusion(bf16[1,2,1536,128]{3,2,1,0:T(8,128)(2,1)} %bitcast.51, f32[2,8,1536]{2,1,0:T(8,128)S(1)} %reshape.98, f32[2,8,1536]{2,1,0:T(8,128)S(1)} %fusion.1, f32[2,8,12]{1,2,0:T(8,128)S(1)} %copy.35), kind=kOutput, calls=%fused_computation.6 | convolution fusion | flops 3613696 | bytes 985856 | tf_op jit(solution)/shard_map/bhgs,bhsd->bhgd/dot_general | solution.py:49
  (2 shorter events, 0.0 us)
Async XLA Ops:
  7.2 26.4 %copy-start = (bf16[4,192,2048]{2,1,0:T(8,128)(2,1)S(1)}, bf16[4,192,2048]{2,1,0:T(8,128)(2,1)}, u32[]{:S(2)}) copy-start(bf16[4,192,2048]{2,1,0:T(8,128)(2,1)} %param.5) | copy-start | bytes 9437188
  7.2 26.4 %all-gather.5.cloned.1.call-start = ((), (), s32[]{:S(2)}) async-start(), calls=%async_computation.3 | async-start | bytes 1572864 | tf_op jit(solution)/shard_map/all_gather | solution.py:22
  7.9 48.5 %all-gather.3.cloned.1.call-start = ((), (), s32[]{:S(2)}) async-start(), calls=%async_computation.2 | async-start | bytes 1572864 | tf_op jit(solution)/shard_map/all_gather | solution.py:17
  64.8 23.3 %copy-start.3 = (f32[32]{0:T(128)S(1)}, f32[32]{0:T(128)}, u32[]{:S(2)}) copy-start(f32[32]{0:T(128)} %param.9) | copy-start | bytes 388
  67.1 41.5 %copy-start.2 = (bf16[1,16,64]{2,1,0:T(8,128)(2,1)S(1)}, bf16[1,16,64]{2,1,0:T(8,128)(2,1)}, u32[]{:S(2)}) copy-start(bf16[1,16,64]{2,1,0:T(8,128)(2,1)} %param.8) | copy-start | bytes 6148
  82.6 24.8 %all-to-all-start.1 = ((bf16[8,2,192,128]{3,2,1,0:T(8,128)(2,1)}), bf16[8,2,192,128]{3,2,1,0:T(8,128)(2,1)}, u32[]{:S(2)}, u32[]{:S(2)}) async-start(bf16[8,2,192,128]{3,2,1,0:T(8,128)(2,1)} %bitcast.48), calls=%async_computation.1 | async-start | bytes 1572864 | tf_op jit(solution)/shard_map/all_to_all | solution.py:30
  108.6 0.9 copy-start.1
Sparse Core Ops, SparseCore 0:
  9.5 23.9 all-gather.4
  35.1 21.2 all-gather.2
where the time goes:
time: 140 us; the launch traced here: 139 us
  waiting for transfers between devices  62.9 us (45%)
  other arithmetic  23.2 us (17%)
  blocking collectives  14.5 us (10%)
  between operations  14.1 us (10%)
  local copies, waits for them, and re-layouts  10.3 us (7%)
  matrix products  8.45 us (6%)
  starting transfers between devices  5.59 us (4%)
    all_gather x1, waiting for transfers between devices, local(): lax.all_gather(content_projection_matrix, 'tp', axis=0, tiled=True)  24.9 us
    another operation x2, other arithmetic  20.2 us
    all_to_all x1, waiting for transfers between devices, local(): lax.all_to_all(spread, 'sp', split_axis=0, concat_axis=2, tiled=True)  19.2 us
    all_gather x1, waiting for transfers between devices, local(): lax.all_gather(key_weight, 'tp', axis=0, tiled=True)  17.5 us
    all_to_all x1, blocking collectives, local(): lax.all_to_all(spread, 'tp', split_axis=1, concat_axis=0, tiled=True)  14.5 us
    all_to_all x1, starting transfers between devices, local(): lax.all_to_all(spread, 'sp', split_axis=0, concat_axis=2, tiled=True)  5.52 us
    dot_general x1, matrix products, local(): jnp.dot(input_rows, lax.all_gather(key_weight, 'tp', axis=0, tiled=True),...  2.96 us
    dot_general x1, matrix products, local(): jnp.dot(input_rows, lax.all_gather(content_projection_matrix, 'tp', axis=...  2.95 us
  transfers between devices with their start and end apart: 3, of which 3 were waited for; matrix products, arithmetic and copies ran while one was open for 4% of the time, Pallas kernels for 0%

commit v1 on v0

v1 whole, which is shorter than its diff:
```python
import functools

import jax
import jax.numpy as jnp
from jax import lax
from jax.experimental import pallas as pl
from jax.experimental.pallas import tpu as pltpu
from jax.sharding import PartitionSpec as P

HEAD_DIM = 64
LANES = 128
MESH = pl.DeviceIdType.MESH


def kernel(
    sizes, x_hbm, k_hbm, v_hbm, q_ref, off_ref, cache_hbm, att_ref,
    x, w, acc, send, recv, x_sem, w_sem,
    s1, r1, s2, r2, s3, r3, s4, r4, out_sem,
):
    groups, spread, heads_dev, pair = sizes
    g, s, t = lax.axis_index("gr"), lax.axis_index("sp"), lax.axis_index("tp")
    seqs, block, width = x.shape
    rows = width // heads_dev
    piece = rows // (groups * pair)
    key_heads = send.shape[1]
    seq_local, slots, span = recv.shape[:3]
    copies = max(1, heads_dev // key_heads)
    side = lax.rem(s, pair)
    mate = s - side + lax.rem(side + 1, pair)

    w_loads = []
    for m, ref in enumerate((k_hbm, v_hbm)):
        load = pltpu.make_async_copy(
            ref, w.at[m, pl.ds(pl.multiple_of(t * rows, 8), rows)], w_sem.at[m]
        )
        load.start()
        w_loads.append(load)
    x_loads = []
    for i in range(seqs):
        load = pltpu.make_async_copy(x_hbm.at[i], x.at[i], x_sem.at[i])
        load.start()
        x_loads.append(load)

    barrier = pltpu.get_barrier_semaphore()
    members = spread * heads_dev
    me = s * heads_dev + t

    def greet(k, carry):
        other = lax.rem(me + k, members)
        pl.semaphore_signal(
            barrier, inc=1, device_id=(g, other // heads_dev, lax.rem(other, heads_dev)),
            device_id_type=MESH,
        )
        return carry

    lax.fori_loop(1, members, greet, 0)
    for k in range(1, groups):
        pl.semaphore_signal(
            barrier, inc=1, device_id=(lax.rem(g + k, groups), s, t), device_id_type=MESH
        )
    pl.semaphore_wait(barrier, members - 1 + groups - 1)

    def part(m, owner, group, half):
        start = pl.multiple_of(owner * rows + (group * pair + half) * piece, 8)
        return w.at[m, pl.ds(start, piece)]

    def remote(ref, send_sem, recv_sem, device):
        return pltpu.make_async_remote_copy(
            src_ref=ref, dst_ref=ref, send_sem=send_sem, recv_sem=recv_sem,
            device_id=device, device_id_type=MESH,
        )

    sent = []
    for m in range(2):
        w_loads[m].wait()
        for d in range(1, heads_dev):
            copy = remote(
                part(m, t, g, side), s1.at[m, d - 1], r1.at[m, d - 1],
                (g, s, lax.rem(t + d, heads_dev)),
            )
            copy.start()
            sent.append(copy)

    own = pl.ds(pl.multiple_of(t * rows, LANES), rows)
    half_cols = w.shape[2]

    def own_product(i):
        for m in range(2):
            acc[i, :, m * half_cols:(m + 1) * half_cols] = jnp.dot(
                x[i, :, own], w[m, own], preferred_element_type=jnp.float32
            )

    for i in range(seqs):
        x_loads[i].wait()
    own_product(0)

    for m in range(2):
        for d in range(1, heads_dev):
            owner = lax.rem(t + heads_dev - d, heads_dev)
            here = part(m, owner, g, side)
            remote(here, s1.at[m, d - 1], r1.at[m, d - 1], (g, s, t)).wait_recv()
            if pair > 1:
                copy = remote(here, s2.at[m, d - 1], r2.at[m, d - 1], (g, mate, t))
                copy.start()
                sent.append(copy)
            for k in range(1, groups):
                copy = remote(
                    here, s3.at[m, d - 1, 0, k - 1], r3.at[m, d - 1, 0, k - 1],
                    (lax.rem(g + k, groups), s, t),
                )
                copy.start()
                sent.append(copy)
        if m == 0:
            for i in range(1, seqs):
                own_product(i)
    if pair > 1:
        for m in range(2):
            for d in range(1, heads_dev):
                owner = lax.rem(t + heads_dev - d, heads_dev)
                there = part(m, owner, g, 1 - side)
                remote(there, s2.at[m, d - 1], r2.at[m, d - 1], (g, mate, t)).wait_recv()
                for k in range(1, groups):
                    copy = remote(
                        there, s3.at[m, d - 1, 1, k - 1], r3.at[m, d - 1, 1, k - 1],
                        (lax.rem(g + k, groups), s, t),
                    )
                    copy.start()
                    sent.append(copy)
    for m in range(2):
        for d in range(1, heads_dev):
            owner = lax.rem(t + heads_dev - d, heads_dev)
            for k in range(1, groups):
                source = lax.rem(g + groups - k, groups)
                for e in range(pair):
                    half = side if e == 0 else 1 - side
                    remote(
                        part(m, owner, source, half),
                        s3.at[m, d - 1, e, k - 1], r3.at[m, d - 1, e, k - 1],
                        (source, s, t),
                    ).wait_recv()

    def message(i, k):
        to = lax.rem(t + k, heads_dev)
        seq = t * seqs + i
        dst_s = seq // seq_local
        src = send.at[i, pl.ds(to * slots // copies, slots)]
        dst = recv.at[lax.rem(seq, seq_local), :, pl.ds(pl.multiple_of(s * block, 8), block)]
        return to, dst_s, src, dst, lax.rem(seq, seq_local)

    for i in range(seqs):
        total = []
        for m in range(2):
            value = acc[i, :, m * half_cols:(m + 1) * half_cols]
            for d in range(1, heads_dev):
                owner = lax.rem(t + d, heads_dev)
                cut = pl.ds(pl.multiple_of(owner * rows, LANES), rows)
                value = value + jnp.dot(
                    x[i, :, cut], w[m, cut], preferred_element_type=jnp.float32
                )
            total.append(value.astype(jnp.bfloat16))
        for h in range(key_heads):
            cut = slice(h * HEAD_DIM, (h + 1) * HEAD_DIM)
            send[i, h] = jnp.concatenate([total[0][:, cut], total[1][:, cut]], axis=1)
        for k in list(range(1, heads_dev)) + [0]:
            to, dst_s, src, dst, ql = message(i, k)
            local = jnp.logical_and(dst_s == s, to == t)

            @pl.when(local)
            def _():
                pltpu.make_async_copy(src, dst, r4.at[ql, s]).start()

            @pl.when(jnp.logical_not(local))
            def _():
                pltpu.make_async_remote_copy(
                    src_ref=src, dst_ref=dst, send_sem=s4.at[i, k], recv_sem=r4.at[ql, s],
                    device_id=(g, dst_s, to), device_id_type=MESH,
                ).start()

    for ql in range(seq_local):
        for b in range(spread):
            landed = recv.at[ql, :, pl.ds(b * block, block)]
            pltpu.make_async_copy(landed, landed, r4.at[ql, b]).wait()
            pltpu.make_async_copy(
                landed, cache_hbm.at[ql, :, pl.ds(b * block, block)], out_sem.at[ql, b]
            ).start()

    head_local = q_ref.shape[1]
    per_slot = head_local // slots
    row_id = lax.broadcasted_iota(jnp.int32, (per_slot, 1), 0)
    lane = lax.broadcasted_iota(jnp.int32, (per_slot, LANES), 1)
    for ql in range(seq_local):
        for u in range(slots):
            offset = jnp.zeros((per_slot, 1), jnp.float32)
            for j in range(per_slot):
                offset = jnp.where(
                    row_id == j, off_ref[t * head_local + u * per_slot + j], offset
                )
            q = q_ref[ql, u * per_slot:(u + 1) * per_slot, :]
            q = jnp.concatenate([q, jnp.zeros_like(q)], axis=1)
            later = jnp.zeros((per_slot, 1), jnp.float32)
            z = lax.dot_general(
                q, recv[ql, u], (((1,), (1,)), ((), ())), preferred_element_type=jnp.float32
            ) * HEAD_DIM ** -0.5 + offset
            stay = -(jnp.maximum(z, 0.0) + jnp.log1p(jnp.exp(-jnp.abs(z))))
            parts = []
            for c in range(span // LANES - 1, -1, -1):
                cols = slice(c * LANES, (c + 1) * LANES)
                run = stay[:, cols]
                step = 1
                while step < LANES:
                    moved = pltpu.roll(run, LANES - step, 1)
                    run = run + jnp.where(lane < LANES - step, moved, 0.0)
                    step *= 2
                parts.append(jnp.exp(z[:, cols] + (run + later)).astype(jnp.bfloat16))
                later = later + run[:, 0:1]
            weight = jnp.concatenate(parts[::-1], axis=1)
            result = jnp.dot(weight, recv[ql, u], preferred_element_type=jnp.float32)
            att_ref[ql, u * per_slot:(u + 1) * per_slot, :] = result[:, HEAD_DIM:].astype(
                jnp.bfloat16
            )

    for copy in sent:
        copy.wait_send()
    for i in range(seqs):
        for k in range(heads_dev):
            to, dst_s, src, dst, ql = message(i, k)

            @pl.when(jnp.logical_not(jnp.logical_and(dst_s == s, to == t)))
            def _():
                pltpu.make_async_remote_copy(
                    src_ref=src, dst_ref=dst, send_sem=s4.at[i, k], recv_sem=r4.at[ql, s],
                    device_id=(g, dst_s, to), device_id_type=MESH,
                ).wait_send()
    for ql in range(seq_local):
        for b in range(spread):
            landed = recv.at[ql, :, pl.ds(b * block, block)]
            pltpu.make_async_copy(
                landed, cache_hbm.at[ql, :, pl.ds(b * block, block)], out_sem.at[ql, b]
            ).wait()


def solution(mesh):
    groups, spread, heads_dev = mesh.shape["gr"], mesh.shape["sp"], mesh.shape["tp"]
    pair = 2 if spread % 2 == 0 else 1

    def local(mixer_input, key_weight, content_projection_matrix, new_queries, head_stick_offset):
        seqs, block, width = mixer_input.shape
        cols = key_weight.shape[1]
        key_heads = cols // HEAD_DIM
        seq_local, head_local = new_queries.shape[:2]
        slots = max(key_heads, heads_dev) // heads_dev
        span = block * spread
        others = heads_dev - 1
        dma = pltpu.SemaphoreType.DMA
        hbm = pl.BlockSpec(memory_space=pl.ANY)
        vmem = pl.BlockSpec(memory_space=pltpu.VMEM)
        return pl.pallas_call(
            functools.partial(kernel, (groups, spread, heads_dev, pair)),
            out_shape=(
                jax.ShapeDtypeStruct((seq_local, slots, span, 2 * HEAD_DIM), jnp.bfloat16),
                jax.ShapeDtypeStruct(new_queries.shape, jnp.bfloat16),
            ),
            in_specs=[hbm, hbm, hbm, vmem, pl.BlockSpec(memory_space=pltpu.SMEM)],
            out_specs=(hbm, vmem),
            scratch_shapes=[
                pltpu.VMEM((seqs, block, width), jnp.bfloat16),
                pltpu.VMEM((2, width, cols), jnp.bfloat16),
                pltpu.VMEM((seqs, block, 2 * cols), jnp.float32),
                pltpu.VMEM((seqs, key_heads, block, 2 * HEAD_DIM), jnp.bfloat16),
                pltpu.VMEM((seq_local, slots, span, 2 * HEAD_DIM), jnp.bfloat16),
                dma((seqs,)),
                dma((2,)),
                dma((2, others)),
                dma((2, others)),
                dma((2, others)),
                dma((2, others)),
                dma((2, others, 2, groups - 1)),
                dma((2, others, 2, groups - 1)),
                dma((seqs, heads_dev)),
                dma((seq_local, spread)),
                dma((seq_local, spread)),
            ],
            compiler_params=pltpu.CompilerParams(collective_id=0, has_side_effects=True),
        )(mixer_input, key_weight, content_projection_matrix, new_queries, head_stick_offset)

    return jax.shard_map(
        local,
        mesh=mesh,
        in_specs=(
            P(("gr", "tp"), "sp", None),
            P("tp", None),
            P("tp", None),
            P(("gr", "sp"), "tp", None),
            P(),
        ),
        out_specs=(P(("gr", "sp"), "tp", None, None), P(("gr", "sp"), "tp", None)),
        check_vma=False,
    )
```

time: 140 us -> 61.2 us (0.44)
  the two profiles are of different devices: /device:TPU:0 before, /device:TPU:29 now
where the time goes in v1:
time: 61.2 us; the launch traced here: 60.4 us
  Pallas kernels  56.5 us (92%)
  local copies, waits for them, and re-layouts  3.33 us (5%)
  between operations  0.64 us (1%)
    pallas_call x1, Pallas kernels, local(): pl.pallas_call(functools.partial(kernel, (groups, spread, heads_dev, pair...  56.5 us
    unnamed x2, local copies, waits for them, and re-layouts  3.33 us

profile of v1, /device:TPU:29, one launch (start us, length us, event | category | flops | bytes accessed | tf_op | source)
XLA Modules:
  0.0 60.4 jit_solution(17149148553052725625)
XLA Ops:
  0.6 56.5 %shard_map.68 = (bf16[1,2,1536,128]{3,2,1,0:T(8,128)(2,1)}, bf16[1,16,64]{2,1,0:T(8,128)(2,1)}) custom-call(bf16[4,192,2048]{2,1,0:T(8,128)(2,1)} %x_hbm.1, bf16[1024,256]{1,0:T(8,128)(2,1)} %k_hbm.1, bf16[1024,256]{1,0:T(8,128)(2,1)} %v_hbm.1, bf16[1,16,64]{2,1,0:T(8,128)(2,1)} %q_ref.1, f32[32]{0:T(128)} %off_ref.1), custom_call_target="tpu_custom_call" | custom-call | tf_op jit(solution)/shard_map/pallas_call | solution.py:257
  57.1 2.1 %copy.9 = bf16[1,2,1536,128]{3,2,1,0:T(8,128)(2,1)} copy(bf16[1,2,1536,128]{3,2,1,0:T(8,128)(2,1)} %get-tuple-element.4) | data formatting | bytes 1572864
  59.2 1.3 %copy.10 = bf16[1,16,64]{2,1,0:T(8,128)(2,1)} copy(bf16[1,16,64]{2,1,0:T(8,128)(2,1)} %get-tuple-element.5) | data formatting | bytes 4096

commit v2 on v1

--- a/solution.py
+++ b/solution.py
@@ -14,8 +14,8 @@
 
 def kernel(
     sizes, x_hbm, k_hbm, v_hbm, q_ref, off_ref, cache_hbm, att_ref,
-    x, w, acc, send, recv, x_sem, w_sem,
-    s1, r1, s2, r2, s3, r3, s4, r4, out_sem,
+    x, w, acc, send, stage, recv, x_sem, w_sem,
+    s1, r1, s2, r2, s3, r3, s4, r4, s5, r5, out_sem,
 ):
     groups, spread, heads_dev, pair = sizes
     g, s, t = lax.axis_index("gr"), lax.axis_index("sp"), lax.axis_index("tp")
@@ -139,13 +139,31 @@
                         (source, s, t),
                     ).wait_recv()
 
-    def message(i, k):
+    def onward(k, i):
+        seq = lax.rem(t + heads_dev - k, heads_dev) * seqs + i
+        ql, dst_s = lax.rem(seq, seq_local), seq // seq_local
+        src = send.at[i, pl.ds(t * slots // copies, slots)] if k == 0 else stage.at[k - 1, i]
+        dst = recv.at[ql, :, pl.ds(pl.multiple_of(s * block, 8), block)]
+        stays = dst_s == s
+        inside = pltpu.make_async_copy(src, dst, r4.at[ql, s])
+        outside = pltpu.make_async_remote_copy(
+            src_ref=src, dst_ref=dst, send_sem=s4.at[k, i], recv_sem=r4.at[ql, s],
+            device_id=(g, dst_s, t), device_id_type=MESH,
+        )
+        return stays, inside, outside
+
+    def start_onward(k, i):
+        stays, inside, outside = onward(k, i)
+        pl.when(stays)(inside.start)
+        pl.when(jnp.logical_not(stays))(outside.start)
+
+    def across(k, i):
         to = lax.rem(t + k, heads_dev)
-        seq = t * seqs + i
-        dst_s = seq // seq_local
-        src = send.at[i, pl.ds(to * slots // copies, slots)]
-        dst = recv.at[lax.rem(seq, seq_local), :, pl.ds(pl.multiple_of(s * block, 8), block)]
-        return to, dst_s, src, dst, lax.rem(seq, seq_local)
+        return pltpu.make_async_remote_copy(
+            src_ref=send.at[i, pl.ds(to * slots // copies, slots)], dst_ref=stage.at[k - 1, i],
+            send_sem=s5.at[k - 1, i], recv_sem=r5.at[k - 1, i],
+            device_id=(g, s, to), device_id_type=MESH,
+        )
 
     for i in range(seqs):
         total = []
@@ -161,20 +179,13 @@
         for h in range(key_heads):
             cut = slice(h * HEAD_DIM, (h + 1) * HEAD_DIM)
             send[i, h] = jnp.concatenate([total[0][:, cut], total[1][:, cut]], axis=1)
-        for k in list(range(1, heads_dev)) + [0]:
-            to, dst_s, src, dst, ql = message(i, k)
-            local = jnp.logical_and(dst_s == s, to == t)
-
-            @pl.when(local)
-            def _():
-                pltpu.make_async_copy(src, dst, r4.at[ql, s]).start()
-
-            @pl.when(jnp.logical_not(local))
-            def _():
-                pltpu.make_async_remote_copy(
-                    src_ref=src, dst_ref=dst, send_sem=s4.at[i, k], recv_sem=r4.at[ql, s],
-                    device_id=(g, dst_s, to), device_id_type=MESH,
-                ).start()
+        for k in range(1, heads_dev):
+            across(k, i).start()
+        start_onward(0, i)
+    for i in range(seqs):
+        for k in range(1, heads_dev):
+            across(k, i).wait_recv()
+            start_onward(k, i)
 
     for ql in range(seq_local):
         for b in range(spread):
@@ -223,14 +234,10 @@
         copy.wait_send()
     for i in range(seqs):
         for k in range(heads_dev):
-            to, dst_s, src, dst, ql = message(i, k)
-
-            @pl.when(jnp.logical_not(jnp.logical_and(dst_s == s, to == t)))
-            def _():
-                pltpu.make_async_remote_copy(
-                    src_ref=src, dst_ref=dst, send_sem=s4.at[i, k], recv_sem=r4.at[ql, s],
-                    device_id=(g, dst_s, to), device_id_type=MESH,
-                ).wait_send()
+            stays, inside, outside = onward(k, i)
+            pl.when(jnp.logical_not(stays))(outside.wait_send)
+            if k > 0:
+                across(k, i).wait_send()
     for ql in range(seq_local):
         for b in range(spread):
             landed = recv.at[ql, :, pl.ds(b * block, block)]
@@ -267,6 +274,7 @@
                 pltpu.VMEM((2, width, cols), jnp.bfloat16),
                 pltpu.VMEM((seqs, block, 2 * cols), jnp.float32),
                 pltpu.VMEM((seqs, key_heads, block, 2 * HEAD_DIM), jnp.bfloat16),
+                pltpu.VMEM((others, seqs, slots, block, 2 * HEAD_DIM), jnp.bfloat16),
                 pltpu.VMEM((seq_local, slots, span, 2 * HEAD_DIM), jnp.bfloat16),
                 dma((seqs,)),
                 dma((2,)),
@@ -276,8 +284,10 @@
                 dma((2, others)),
                 dma((2, others, 2, groups - 1)),
                 dma((2, others, 2, groups - 1)),
-                dma((seqs, heads_dev)),
+                dma((heads_dev, seqs)),
                 dma((seq_local, spread)),
+                dma((others, seqs)),
+                dma((others, seqs)),
                 dma((seq_local, spread)),
             ],
             compiler_params=pltpu.CompilerParams(collective_id=0, has_side_effects=True),

time: 61.2 us -> 47.5 us (0.78)
  Pallas kernels: 56.5 us -> 43.3 us
    pallas_call x1, Pallas kernels: 56.5 us -> 43.3 us  [local(): pl.pallas_call(functools.partial(kernel, (groups, spread, heads_dev, pair...]
where the time goes in v2:
time: 47.5 us; the launch traced here: 47.3 us
  Pallas kernels  43.3 us (91%)
  local copies, waits for them, and re-layouts  3.33 us (7%)
  between operations  0.64 us (1%)
    pallas_call x1, Pallas kernels, local(): pl.pallas_call(functools.partial(kernel, (groups, spread, heads_dev, pair...  43.3 us
    unnamed x2, local copies, waits for them, and re-layouts  3.33 us

profile of v2, /device:TPU:29, one launch (start us, length us, event | category | flops | bytes accessed | tf_op | source)
XLA Modules:
  0.0 47.3 jit_solution(7753616061706762232)
XLA Ops:
  0.6 43.3 %shard_map.68 = (bf16[1,2,1536,128]{3,2,1,0:T(8,128)(2,1)}, bf16[1,16,64]{2,1,0:T(8,128)(2,1)}) custom-call(bf16[4,192,2048]{2,1,0:T(8,128)(2,1)} %x_hbm.1, bf16[1024,256]{1,0:T(8,128)(2,1)} %k_hbm.1, bf16[1024,256]{1,0:T(8,128)(2,1)} %v_hbm.1, bf16[1,16,64]{2,1,0:T(8,128)(2,1)} %q_ref.1, f32[32]{0:T(128)} %off_ref.1), custom_call_target="tpu_custom_call" | custom-call | tf_op jit(solution)/shard_map/pallas_call | solution.py:264
  43.9 2.1 %copy.9 = bf16[1,2,1536,128]{3,2,1,0:T(8,128)(2,1)} copy(bf16[1,2,1536,128]{3,2,1,0:T(8,128)(2,1)} %get-tuple-element.4) | data formatting | bytes 1572864
  46.0 1.3 %copy.10 = bf16[1,16,64]{2,1,0:T(8,128)(2,1)} copy(bf16[1,16,64]{2,1,0:T(8,128)(2,1)} %get-tuple-element.5) | data formatting | bytes 4096

commit v3 on v2

--- a/solution.py
+++ b/solution.py
@@ -9,6 +9,7 @@
 
 HEAD_DIM = 64
 LANES = 128
+CUTS = 2
 MESH = pl.DeviceIdType.MESH
 
 
@@ -28,13 +29,23 @@
     side = lax.rem(s, pair)
     mate = s - side + lax.rem(side + 1, pair)
 
+    chunks, _, chunk_cols = w.shape
+    wide = chunk_cols // 2
+    chunk_heads = wide // HEAD_DIM
+
+    def first(owner, e):
+        return lax.rem((owner + 1) * slots // copies // chunk_heads + e, chunks)
+
+    own_rows = pl.ds(pl.multiple_of(t * rows, LANES), rows)
     w_loads = []
-    for m, ref in enumerate((k_hbm, v_hbm)):
-        load = pltpu.make_async_copy(
-            ref, w.at[m, pl.ds(pl.multiple_of(t * rows, 8), rows)], w_sem.at[m]
-        )
-        load.start()
-        w_loads.append(load)
+    for c in range(chunks):
+        for m, ref in enumerate((k_hbm, v_hbm)):
+            load = pltpu.make_async_copy(
+                ref.at[:, pl.ds(c * wide, wide)],
+                w.at[c, own_rows, pl.ds(m * wide, wide)], w_sem.at[c, m],
+            )
+            load.start()
+            w_loads.append(load)
     x_loads = []
     for i in range(seqs):
         load = pltpu.make_async_copy(x_hbm.at[i], x.at[i], x_sem.at[i])
@@ -60,9 +71,9 @@
         )
     pl.semaphore_wait(barrier, members - 1 + groups - 1)
 
-    def part(m, owner, group, half):
-        start = pl.multiple_of(owner * rows + (group * pair + half) * piece, 8)
-        return w.at[m, pl.ds(start, piece)]
+    def part(c, owner, group, half, f):
+        start = owner * rows + (group * pair + half) * piece + f * (piece // CUTS)
+        return w.at[c, pl.ds(pl.multiple_of(start, 8), piece // CUTS)]
 
     def remote(ref, send_sem, recv_sem, device):
         return pltpu.make_async_remote_copy(
@@ -71,73 +82,73 @@
         )
 
     sent = []
-    for m in range(2):
-        w_loads[m].wait()
-        for d in range(1, heads_dev):
+    for load in w_loads:
+        load.wait()
+    for e in range(chunks):
+        for f in range(CUTS):
+            for d in range(1, heads_dev):
+                to = lax.rem(t + d, heads_dev)
+                copy = remote(
+                    part(first(to, e), t, g, side, f), s1.at[e, f, d - 1], r1.at[e, f, d - 1],
+                    (g, s, to),
+                )
+                copy.start()
+                sent.append(copy)
+
+    def owner_of(d):
+        return lax.rem(t + heads_dev - d, heads_dev)
+
+    def spread_piece(e, f, d, half, h):
+        ref = part(first(t, e), owner_of(d), g, half, f)
+        for k in range(1, groups):
             copy = remote(
-                part(m, t, g, side), s1.at[m, d - 1], r1.at[m, d - 1],
-                (g, s, lax.rem(t + d, heads_dev)),
+                ref, s3.at[e, f, d - 1, h, k - 1], r3.at[e, f, d - 1, h, k - 1],
+                (lax.rem(g + k, groups), s, t),
             )
             copy.start()
             sent.append(copy)
 
-    own = pl.ds(pl.multiple_of(t * rows, LANES), rows)
-    half_cols = w.shape[2]
-
-    def own_product(i):
-        for m in range(2):
-            acc[i, :, m * half_cols:(m + 1) * half_cols] = jnp.dot(
-                x[i, :, own], w[m, own], preferred_element_type=jnp.float32
+    def pass_first(e):
+        for f in range(CUTS):
+            for d in range(1, heads_dev):
+                here = part(first(t, e), owner_of(d), g, side, f)
+                remote(here, s1.at[e, f, d - 1], r1.at[e, f, d - 1], (g, s, t)).wait_recv()
+                if pair > 1:
+                    copy = remote(here, s2.at[e, f, d - 1], r2.at[e, f, d - 1], (g, mate, t))
+                    copy.start()
+                    sent.append(copy)
+                spread_piece(e, f, d, side, 0)
+
+    def pass_second(e):
+        if pair > 1:
+            for f in range(CUTS):
+                for d in range(1, heads_dev):
+                    there = part(first(t, e), owner_of(d), g, 1 - side, f)
+                    remote(there, s2.at[e, f, d - 1], r2.at[e, f, d - 1], (g, mate, t)).wait_recv()
+                    spread_piece(e, f, d, 1 - side, 1)
+
+    def pass_last(e):
+        for f in range(CUTS):
+            for d in range(1, heads_dev):
+                for k in range(1, groups):
+                    source = lax.rem(g + groups - k, groups)
+                    for h in range(pair):
+                        remote(
+                            part(first(t, e), owner_of(d), source, side if h == 0 else 1 - side, f),
+                            s3.at[e, f, d - 1, h, k - 1], r3.at[e, f, d - 1, h, k - 1],
+                            (source, s, t),
+                        ).wait_recv()
+
+    def own_product(e):
+        for i in range(seqs):
+            acc[e, i] = jnp.dot(
+                x[i, :, own_rows], w[first(t, e), own_rows], preferred_element_type=jnp.float32
             )
 
     for i in range(seqs):
         x_loads[i].wait()
-    own_product(0)
-
-    for m in range(2):
-        for d in range(1, heads_dev):
-            owner = lax.rem(t + heads_dev - d, heads_dev)
-            here = part(m, owner, g, side)
-            remote(here, s1.at[m, d - 1], r1.at[m, d - 1], (g, s, t)).wait_recv()
-            if pair > 1:
-                copy = remote(here, s2.at[m, d - 1], r2.at[m, d - 1], (g, mate, t))
-                copy.start()
-                sent.append(copy)
-            for k in range(1, groups):
-                copy = remote(
-                    here, s3.at[m, d - 1, 0, k - 1], r3.at[m, d - 1, 0, k - 1],
-                    (lax.rem(g + k, groups), s, t),
-                )
-                copy.start()
-                sent.append(copy)
-        if m == 0:
-            for i in range(1, seqs):
-                own_product(i)
-    if pair > 1:
-        for m in range(2):
-            for d in range(1, heads_dev):
-                owner = lax.rem(t + heads_dev - d, heads_dev)
-                there = part(m, owner, g, 1 - side)
-                remote(there, s2.at[m, d - 1], r2.at[m, d - 1], (g, mate, t)).wait_recv()
-                for k in range(1, groups):
-                    copy = remote(
-                        there, s3.at[m, d - 1, 1, k - 1], r3.at[m, d - 1, 1, k - 1],
-                        (lax.rem(g + k, groups), s, t),
-                    )
-                    copy.start()
-                    sent.append(copy)
-    for m in range(2):
-        for d in range(1, heads_dev):
-            owner = lax.rem(t + heads_dev - d, heads_dev)
-            for k in range(1, groups):
-                source = lax.rem(g + groups - k, groups)
-                for e in range(pair):
-                    half = side if e == 0 else 1 - side
-                    remote(
-                        part(m, owner, source, half),
-                        s3.at[m, d - 1, e, k - 1], r3.at[m, d - 1, e, k - 1],
-                        (source, s, t),
-                    ).wait_recv()
+    for e in range(chunks):
+        own_product(e)
 
     def onward(k, i):
         seq = lax.rem(t + heads_dev - k, heads_dev) * seqs + i
@@ -165,23 +176,38 @@
             device_id=(g, s, to), device_id_type=MESH,
         )
 
-    for i in range(seqs):
-        total = []
-        for m in range(2):
-            value = acc[i, :, m * half_cols:(m + 1) * half_cols]
+    def finish(e):
+        c = first(t, e)
+        for i in range(seqs):
+            value = acc[e, i]
             for d in range(1, heads_dev):
-                owner = lax.rem(t + d, heads_dev)
-                cut = pl.ds(pl.multiple_of(owner * rows, LANES), rows)
+                cut = pl.ds(pl.multiple_of(lax.rem(t + d, heads_dev) * rows, LANES), rows)
                 value = value + jnp.dot(
-                    x[i, :, cut], w[m, cut], preferred_element_type=jnp.float32
+                    x[i, :, cut], w[c, cut], preferred_element_type=jnp.float32
                 )
-            total.append(value.astype(jnp.bfloat16))
-        for h in range(key_heads):
-            cut = slice(h * HEAD_DIM, (h + 1) * HEAD_DIM)
-            send[i, h] = jnp.concatenate([total[0][:, cut], total[1][:, cut]], axis=1)
-        for k in range(1, heads_dev):
-            across(k, i).start()
-        start_onward(0, i)
+            value = value.astype(jnp.bfloat16)
+            for h in range(chunk_heads):
+                low = h * HEAD_DIM
+                send[i, c * chunk_heads + h] = jnp.concatenate(
+                    [value[:, low:low + HEAD_DIM], value[:, wide + low:wide + low + HEAD_DIM]],
+                    axis=1,
+                )
+            for k in list(range(1, heads_dev)) + [0]:
+                to = lax.rem(t + k, heads_dev)
+
+                @pl.when(to * slots // copies // chunk_heads == c)
+                def _():
+                    if k:
+                        across(k, i).start()
+                    else:
+                        start_onward(0, i)
+
+    for e in range(chunks):
+        pass_first(e)
+    for e in range(chunks):
+        pass_second(e)
+        pass_last(e)
+        finish(e)
     for i in range(seqs):
         for k in range(1, heads_dev):
             across(k, i).wait_recv()
@@ -258,6 +284,8 @@
         slots = max(key_heads, heads_dev) // heads_dev
         span = block * spread
         others = heads_dev - 1
+        wide = max(LANES, slots * HEAD_DIM)
+        chunks = cols // wide
         dma = pltpu.SemaphoreType.DMA
         hbm = pl.BlockSpec(memory_space=pl.ANY)
         vmem = pl.BlockSpec(memory_space=pltpu.VMEM)
@@ -271,19 +299,19 @@
             out_specs=(hbm, vmem),
             scratch_shapes=[
                 pltpu.VMEM((seqs, block, width), jnp.bfloat16),
-                pltpu.VMEM((2, width, cols), jnp.bfloat16),
-                pltpu.VMEM((seqs, block, 2 * cols), jnp.float32),
+                pltpu.VMEM((chunks, width, 2 * wide), jnp.bfloat16),
+                pltpu.VMEM((chunks, seqs, block, 2 * wide), jnp.float32),
                 pltpu.VMEM((seqs, key_heads, block, 2 * HEAD_DIM), jnp.bfloat16),
                 pltpu.VMEM((others, seqs, slots, block, 2 * HEAD_DIM), jnp.bfloat16),
                 pltpu.VMEM((seq_local, slots, span, 2 * HEAD_DIM), jnp.bfloat16),
                 dma((seqs,)),
-                dma((2,)),
-                dma((2, others)),
-                dma((2, others)),
-                dma((2, others)),
-                dma((2, others)),
-                dma((2, others, 2, groups - 1)),
-                dma((2, others, 2, groups - 1)),
+                dma((chunks, 2)),
+                dma((chunks, CUTS, others)),
+                dma((chunks, CUTS, others)),
+                dma((chunks, CUTS, others)),
+                dma((chunks, CUTS, others)),
+                dma((chunks, CUTS, others, 2, groups - 1)),
+                dma((chunks, CUTS, others, 2, groups - 1)),
                 dma((heads_dev, seqs)),
                 dma((seq_local, spread)),
                 dma((others, seqs)),

time: 47.5 us -> 45.6 us (0.960)
  Pallas kernels: 43.3 us -> 41.4 us
    pallas_call x1, Pallas kernels: 43.3 us -> 41.4 us  [local(): pl.pallas_call(functools.partial(kernel, (groups, spread, heads_dev, pair...]
where the time goes in v3:
time: 45.6 us; the launch traced here: 45.4 us
  Pallas kernels  41.4 us (91%)
  local copies, waits for them, and re-layouts  3.33 us (7%)
  between operations  0.64 us (1%)
    pallas_call x1, Pallas kernels, local(): pl.pallas_call(functools.partial(kernel, (groups, spread, heads_dev, pair...  41.4 us
    unnamed x2, local copies, waits for them, and re-layouts  3.33 us

profile of v3, /device:TPU:29, one launch (start us, length us, event | category | flops | bytes accessed | tf_op | source)
XLA Modules:
  0.0 45.4 jit_solution(7437166063477282718)
XLA Ops:
  0.6 41.4 %shard_map.68 = (bf16[1,2,1536,128]{3,2,1,0:T(8,128)(2,1)}, bf16[1,16,64]{2,1,0:T(8,128)(2,1)}) custom-call(bf16[4,192,2048]{2,1,0:T(8,128)(2,1)} %x_hbm.1, bf16[1024,256]{1,0:T(8,128)(2,1)} %k_hbm.1, bf16[1024,256]{1,0:T(8,128)(2,1)} %v_hbm.1, bf16[1,16,64]{2,1,0:T(8,128)(2,1)} %q_ref.1, f32[32]{0:T(128)} %off_ref.1), custom_call_target="tpu_custom_call" | custom-call | tf_op jit(solution)/shard_map/pallas_call | solution.py:292
  42.1 2.1 %copy.9 = bf16[1,2,1536,128]{3,2,1,0:T(8,128)(2,1)} copy(bf16[1,2,1536,128]{3,2,1,0:T(8,128)(2,1)} %get-tuple-element.4) | data formatting | bytes 1572864
  44.1 1.3 %copy.10 = bf16[1,16,64]{2,1,0:T(8,128)(2,1)} copy(bf16[1,16,64]{2,1,0:T(8,128)(2,1)} %get-tuple-element.5) | data formatting | bytes 4096

commit v4 on v3

--- a/solution.py
+++ b/solution.py
@@ -14,9 +14,9 @@
 
 
 def kernel(
-    sizes, x_hbm, k_hbm, v_hbm, q_ref, off_ref, cache_hbm, att_ref,
-    x, w, acc, send, stage, recv, x_sem, w_sem,
-    s1, r1, s2, r2, s3, r3, s4, r4, s5, r5, out_sem,
+    sizes, x_hbm, k_hbm, v_hbm, recv,
+    x, w, acc, send, stage, x_sem, w_sem,
+    s1, r1, s2, r2, s3, r3, s4, r4, s5, r5,
 ):
     groups, spread, heads_dev, pair = sizes
     g, s, t = lax.axis_index("gr"), lax.axis_index("sp"), lax.axis_index("tp")
@@ -176,50 +176,62 @@
             device_id=(g, s, to), device_id_type=MESH,
         )
 
-    def finish(e):
+    def finish(e, i):
         c = first(t, e)
-        for i in range(seqs):
-            value = acc[e, i]
-            for d in range(1, heads_dev):
-                cut = pl.ds(pl.multiple_of(lax.rem(t + d, heads_dev) * rows, LANES), rows)
-                value = value + jnp.dot(
-                    x[i, :, cut], w[c, cut], preferred_element_type=jnp.float32
-                )
-            value = value.astype(jnp.bfloat16)
-            for h in range(chunk_heads):
-                low = h * HEAD_DIM
-                send[i, c * chunk_heads + h] = jnp.concatenate(
-                    [value[:, low:low + HEAD_DIM], value[:, wide + low:wide + low + HEAD_DIM]],
-                    axis=1,
-                )
-            for k in list(range(1, heads_dev)) + [0]:
-                to = lax.rem(t + k, heads_dev)
-
-                @pl.when(to * slots // copies // chunk_heads == c)
-                def _():
-                    if k:
-                        across(k, i).start()
-                    else:
-                        start_onward(0, i)
+        value = acc[e, i]
+        for d in range(1, heads_dev):
+            cut = pl.ds(pl.multiple_of(lax.rem(t + d, heads_dev) * rows, LANES), rows)
+            value = value + jnp.dot(
+                x[i, :, cut], w[c, cut], preferred_element_type=jnp.float32
+            )
+        value = value.astype(jnp.bfloat16)
+        for h in range(chunk_heads):
+            low = h * HEAD_DIM
+            send[i, c * chunk_heads + h] = jnp.concatenate(
+                [value[:, low:low + HEAD_DIM], value[:, wide + low:wide + low + HEAD_DIM]],
+                axis=1,
+            )
+        for k in list(range(1, heads_dev)) + [0]:
+            to = lax.rem(t + k, heads_dev)
+
+            @pl.when(to * slots // copies // chunk_heads == c)
+            def _():
+                if k:
+                    across(k, i).start()
+                else:
+                    start_onward(0, i)
 
     for e in range(chunks):
         pass_first(e)
     for e in range(chunks):
         pass_second(e)
         pass_last(e)
-        finish(e)
-    for i in range(seqs):
-        for k in range(1, heads_dev):
-            across(k, i).wait_recv()
-            start_onward(k, i)
+        for i in range(seqs):
+            finish(e, i)
+            if e == chunks - 1:
+                for k in range(1, heads_dev):
+                    across(k, i).wait_recv()
+                    start_onward(k, i)
 
     for ql in range(seq_local):
         for b in range(spread):
             landed = recv.at[ql, :, pl.ds(b * block, block)]
             pltpu.make_async_copy(landed, landed, r4.at[ql, b]).wait()
-            pltpu.make_async_copy(
-                landed, cache_hbm.at[ql, :, pl.ds(b * block, block)], out_sem.at[ql, b]
-            ).start()
+
+    for copy in sent:
+        copy.wait_send()
+    for i in range(seqs):
+        for k in range(heads_dev):
+            stays, inside, outside = onward(k, i)
+            pl.when(jnp.logical_not(stays))(outside.wait_send)
+            if k > 0:
+                across(k, i).wait_send()
+
+def read_kernel(recv, q_ref, off_ref, cache_hbm, att_ref, out_sem):
+    t = lax.axis_index("tp")
+    seq_local, slots, span = recv.shape[:3]
+    keep = pltpu.make_async_copy(recv, cache_hbm, out_sem)
+    keep.start()
 
     head_local = q_ref.shape[1]
     per_slot = head_local // slots
@@ -256,20 +268,7 @@
                 jnp.bfloat16
             )
 
-    for copy in sent:
-        copy.wait_send()
-    for i in range(seqs):
-        for k in range(heads_dev):
-            stays, inside, outside = onward(k, i)
-            pl.when(jnp.logical_not(stays))(outside.wait_send)
-            if k > 0:
-                across(k, i).wait_send()
-    for ql in range(seq_local):
-        for b in range(spread):
-            landed = recv.at[ql, :, pl.ds(b * block, block)]
-            pltpu.make_async_copy(
-                landed, cache_hbm.at[ql, :, pl.ds(b * block, block)], out_sem.at[ql, b]
-            ).wait()
+    keep.wait()
 
 
 def solution(mesh):
@@ -289,21 +288,18 @@
         dma = pltpu.SemaphoreType.DMA
         hbm = pl.BlockSpec(memory_space=pl.ANY)
         vmem = pl.BlockSpec(memory_space=pltpu.VMEM)
-        return pl.pallas_call(
+        cache_shape = (seq_local, slots, span, 2 * HEAD_DIM)
+        landed = pl.pallas_call(
             functools.partial(kernel, (groups, spread, heads_dev, pair)),
-            out_shape=(
-                jax.ShapeDtypeStruct((seq_local, slots, span, 2 * HEAD_DIM), jnp.bfloat16),
-                jax.ShapeDtypeStruct(new_queries.shape, jnp.bfloat16),
-            ),
-            in_specs=[hbm, hbm, hbm, vmem, pl.BlockSpec(memory_space=pltpu.SMEM)],
-            out_specs=(hbm, vmem),
+            out_shape=pltpu.VMEM(cache_shape, jnp.bfloat16),
+            in_specs=[hbm, hbm, hbm],
+            out_specs=vmem,
             scratch_shapes=[
                 pltpu.VMEM((seqs, block, width), jnp.bfloat16),
                 pltpu.VMEM((chunks, width, 2 * wide), jnp.bfloat16),
                 pltpu.VMEM((chunks, seqs, block, 2 * wide), jnp.float32),
                 pltpu.VMEM((seqs, key_heads, block, 2 * HEAD_DIM), jnp.bfloat16),
                 pltpu.VMEM((others, seqs, slots, block, 2 * HEAD_DIM), jnp.bfloat16),
-                pltpu.VMEM((seq_local, slots, span, 2 * HEAD_DIM), jnp.bfloat16),
                 dma((seqs,)),
                 dma((chunks, 2)),
                 dma((chunks, CUTS, others)),
@@ -316,10 +312,22 @@
                 dma((seq_local, spread)),
                 dma((others, seqs)),
                 dma((others, seqs)),
-                dma((seq_local, spread)),
             ],
-            compiler_params=pltpu.CompilerParams(collective_id=0, has_side_effects=True),
-        )(mixer_input, key_weight, content_projection_matrix, new_queries, head_stick_offset)
+            compiler_params=pltpu.CompilerParams(
+                collective_id=0, has_side_effects=True
+            ),
+        )(mixer_input, key_weight, content_projection_matrix)
+        return pl.pallas_call(
+            read_kernel,
+            out_shape=(
+                jax.ShapeDtypeStruct(cache_shape, jnp.bfloat16),
+                jax.ShapeDtypeStruct(new_queries.shape, jnp.bfloat16),
+            ),
+            in_specs=[vmem, vmem, pl.BlockSpec(memory_space=pltpu.SMEM)],
+            out_specs=(hbm, vmem),
+            scratch_shapes=[pltpu.SemaphoreType.DMA],
+            compiler_params=pltpu.CompilerParams(vmem_limit_bytes=16 * 2**20),
+        )(landed, new_queries, head_stick_offset)
 
     return jax.shard_map(
         local,

time: 45.6 us -> 42.4 us (0.930)
  local copies, waits for them, and re-layouts: 3.33 us -> 0.01 us
    unnamed x2 -> x4, local copies, waits for them, and re-layouts: 3.33 us -> 0.01 us
    pallas_call x0 -> x1, Pallas kernels: none -> 3.02 us  [local(): pl.pallas_call(read_kernel, out_shape=(jax.ShapeDtypeStruct(cache_shape,...]
    pallas_call x1, Pallas kernels: 41.4 us -> 38.6 us  [local(): pl.pallas_call(functools.partial(kernel, (groups, spread, heads_dev, pair...]
where the time goes in v4:
time: 42.4 us; the launch traced here: 42.3 us
  Pallas kernels  41.6 us (98%)
  between operations  0.67 us (2%)
    pallas_call x1, Pallas kernels, local(): pl.pallas_call(functools.partial(kernel, (groups, spread, heads_dev, pair...  38.6 us
    pallas_call x1, Pallas kernels, local(): pl.pallas_call(read_kernel, out_shape=(jax.ShapeDtypeStruct(cache_shape,...  3.02 us

profile of v4, /device:TPU:29, one launch (start us, length us, event | category | flops | bytes accessed | tf_op | source)
XLA Modules:
  0.0 42.3 jit_solution(9285984627484928148)
XLA Ops:
  0.6 0.0 copy-start.1
  0.6 0.0 copy-start
  0.7 38.6 %shard_map.68.recv = bf16[1,2,1536,128]{3,2,1,0:T(8,128)(2,1)S(1)} custom-call(bf16[4,192,2048]{2,1,0:T(8,128)(2,1)} %x_hbm.1, bf16[1024,256]{1,0:T(8,128)(2,1)} %k_hbm.1, bf16[1024,256]{1,0:T(8,128)(2,1)} %v_hbm.1), custom_call_target="tpu_custom_call" | custom-call | tf_op jit(solution)/shard_map/pallas_call | solution.py:292
  39.2 0.0 copy-done.1
  39.2 0.0 copy-done
  39.3 3.0 %shard_map.69 = (bf16[1,2,1536,128]{3,2,1,0:T(8,128)(2,1)}, bf16[1,16,64]{2,1,0:T(8,128)(2,1)}) custom-call(bf16[1,2,1536,128]{3,2,1,0:T(8,128)(2,1)S(1)} %shard_map.68.recv, bf16[1,16,64]{2,1,0:T(8,128)(2,1)S(1)} %copy-done, f32[32]{0:T(128)S(1)} %copy-done.1), custom_call_target="tpu_custom_call" | custom-call | tf_op jit(solution)/shard_map/pallas_call | solution.py:320
Async XLA Ops:
  0.6 38.6 %copy-start.1 = (f32[32]{0:T(128)S(1)}, f32[32]{0:T(128)}, u32[]{:S(2)}) copy-start(f32[32]{0:T(128)} %off_ref.1) | copy-start | bytes 388
  0.6 38.6 %copy-start = (bf16[1,16,64]{2,1,0:T(8,128)(2,1)S(1)}, bf16[1,16,64]{2,1,0:T(8,128)(2,1)}, u32[]{:S(2)}) copy-start(bf16[1,16,64]{2,1,0:T(8,128)(2,1)} %q_ref.1) | copy-start | bytes 6148
